TPU v7x, 32 devices: a whole 2x2x4 slice. The times are simulated.
32 devices in a mesh: kv: 8 (over z, y), tp: 4 (over x, core).
Axes of the slice: x: 2, y: 2, z: 4, core: 2. Of those that a mesh axis runs over, the one named last changes fastest.
Arguments:
- residual_entries: bfloat16 [512, 4096], P(None, ('kv', 'tp')), may hold values from -6 to 6
- fresh_extents: int32 [64], replicated, may hold values from 1 to 8, 256 in all
- memory_matrix: float32 [64, 16, 128, 128], P('kv', 'tp'), may hold values from -3 to 3
- initial_rescale_vector: float32 [4096], P('kv'), may hold values from 0.1 to 1.9
- probe_matrix: bfloat16 [4096, 2048], P('kv', 'tp'), may hold values from -0.09375 to 0.09375
- retain_matrix: bfloat16 [4096, 2048], P('kv', 'tp'), may hold values from -0.09375 to 0.09375
- content_matrix: bfloat16 [4096, 2048], P('kv', 'tp'), may hold values from -0.09375 to 0.09375
- result_switch_matrix: bfloat16 [4096, 2048], P('kv', 'tp'), may hold values from -0.09375 to 0.09375
- retain_lower_limit: float32 [2048], P('tp'), may hold values from 0 to 0.9
- extra_shrink_log: float32 [512, 16], P('kv', 'tp'), may hold values from -0.7 to 0
- lane_result_rescale: float32 [128], replicated, may hold values from 0.1 to 1.9
- result_matrix: bfloat16 [2048, 4096], P('tp', 'kv'), may hold values from -0.125 to 0.125
- later_rescale_vector: float32 [4096], P(('kv', 'tp')), may hold values from 0.1 to 1.9
- mixer_switch_matrix: bfloat16 [4096, 11008], P(None, ('kv', 'tp')), may hold values from -0.09375 to 0.09375
- widening_matrix: bfloat16 [4096, 11008], P(None, ('kv', 'tp')), may hold values from -0.09375 to 0.09375
- narrowing_matrix: bfloat16 [11008, 4096], P(('kv', 'tp')), may hold values from -0.109375 to 0.109375
Outputs:
- mixed: bfloat16 [512, 4096], P(None, ('kv', 'tp'))
- new_state: float32 [64, 16, 128, 128], P('kv', 'tp')
Inputs may be any that keep to these rules, and one draw needn't show every extreme that they name: `fresh_extents`: the lengths sum to exactly 256.
All inputs are finite; a program needn't handle non-finite values.
Results may differ from a plain program's by a relative error of at most 0.022.
Values may be sent and summed in bfloat16 or wider, within the bound.
A program may use at most 64 MiB of HBM per device.

v0:
```python
import jax
import jax.numpy as jnp
from jax import lax
from jax.sharding import PartitionSpec as P

D = 4096
HEAD = 128
FRESH_PLACES = 8
epsilon = 1e-06


def local(
    residual_entries,
    fresh_extents,
    memory_matrix,
    initial_rescale_vector,
    probe_matrix,
    retain_matrix,
    content_matrix,
    result_switch_matrix,
    retain_lower_limit,
    extra_shrink_log,
    lane_result_rescale,
    result_matrix,
    later_rescale_vector,
    mixer_switch_matrix,
    widening_matrix,
    narrowing_matrix,
):
    sequences_per_device = memory_matrix.shape[0]
    heads_per_device = memory_matrix.shape[1]
    rows_dev = sequences_per_device * FRESH_PLACES
    all_rows = residual_entries.shape[0]
    kv_index = lax.axis_index("kv")
    tokens_wide = residual_entries.astype(jnp.float32)
    columns = lax.all_gather(residual_entries, "tp", axis=1, tiled=True)
    squares = lax.psum(jnp.sum(tokens_wide * tokens_wide, axis=1), ("kv", "tp"))
    own_squares = lax.dynamic_slice_in_dim(squares, kv_index * rows_dev, rows_dev)
    first_scale = lax.rsqrt(own_squares / D + epsilon)
    scaled = (columns.astype(jnp.float32) * initial_rescale_vector).astype(jnp.bfloat16)
    projected = (
        lax.psum_scatter(
            jnp.concatenate(
                [
                    jnp.dot(scaled, weight, preferred_element_type=jnp.float32)
                    for weight in (
                        probe_matrix,
                        retain_matrix,
                        content_matrix,
                        result_switch_matrix,
                    )
                ],
                axis=1,
            ).astype(jnp.bfloat16),
            "kv",
            scatter_dimension=0,
            tiled=True,
        ).astype(jnp.float32)
        * first_scale[:, None]
    )
    width_dev = probe_matrix.shape[1]
    shape_four = (sequences_per_device, FRESH_PLACES, heads_per_device, HEAD)
    z_query = projected[:, :width_dev]
    z_forget = projected[:, width_dev : 2 * width_dev].reshape(shape_four)
    z_input = projected[:, 2 * width_dev : 3 * width_dev].reshape(shape_four)
    z_outgate = projected[:, 3 * width_dev :]
    own_lengths = lax.dynamic_slice_in_dim(
        fresh_extents, kv_index * sequences_per_device, sequences_per_device
    )
    living = jnp.arange(FRESH_PLACES, dtype=jnp.int32)[None, :] < own_lengths[:, None]
    query = jax.nn.silu(z_query).reshape(shape_four)
    bounds = retain_lower_limit.reshape(heads_per_device, HEAD)
    retain_factor = bounds + (1.0 - bounds) * jax.nn.sigmoid(z_forget)
    shrink_exponent = jnp.log(retain_factor) + extra_shrink_log.reshape(
        sequences_per_device, FRESH_PLACES, heads_per_device, 1
    )
    decays = jnp.where(living[:, :, None, None], jnp.exp(shrink_exponent), 1.0)
    key_gate = jnp.where(living[:, :, None, None], 1.0 - retain_factor, 0.0)
    carried = memory_matrix
    outputs = []
    for position in range(FRESH_PLACES):
        carried = (
            decays[:, position, :, :, None] * carried
            + key_gate[:, position, :, :, None] * z_input[:, position, :, None, :]
        )
        outputs.append(
            jnp.einsum(
                "bhd,bhdv->bhv", query[:, position], carried, precision=lax.Precision.HIGHEST
            )
        )
    heads_out = jnp.stack(outputs, axis=1)
    heads_out = (
        heads_out
        * lax.rsqrt(jnp.mean(heads_out * heads_out, axis=-1, keepdims=True) + epsilon)
        * lane_result_rescale
    )
    normed = jnp.where(
        living.reshape(rows_dev)[:, None],
        heads_out.reshape(rows_dev, width_dev) * jax.nn.silu(z_outgate),
        0.0,
    ).astype(jnp.bfloat16)
    head_partial = jnp.dot(
        lax.all_gather(normed, "kv", axis=0, tiled=True),
        result_matrix,
        preferred_element_type=jnp.float32,
    ).astype(jnp.bfloat16)
    attended = lax.psum_scatter(head_partial, "tp", scatter_dimension=1, tiled=True).astype(
        jnp.float32
    )
    residual = (tokens_wide + attended).astype(jnp.bfloat16)
    resid_wide = residual.astype(jnp.float32)
    resid_squares = lax.psum(jnp.sum(resid_wide * resid_wide, axis=1), ("kv", "tp"))
    second_in = (
        resid_wide * later_rescale_vector * lax.rsqrt(resid_squares / D + epsilon)[:, None]
    ).astype(jnp.bfloat16)
    live_rows = (
        jnp.arange(FRESH_PLACES, dtype=jnp.int32)[None, :] < fresh_extents[:, None]
    ).reshape(all_rows)
    live_order = jnp.argsort(1 - live_rows.astype(jnp.int32), stable=True)[: all_rows // 2]
    mixer_input = jnp.take(second_in, live_order, axis=0)
    piece = lax.all_gather(mixer_input, ("kv", "tp"), axis=1, tiled=True)
    gated = jnp.dot(piece, mixer_switch_matrix, preferred_element_type=jnp.float32)
    upward = jnp.dot(piece, widening_matrix, preferred_element_type=jnp.float32)
    hidden = (jax.nn.silu(gated) * upward).astype(jnp.bfloat16)
    mixer_terms = lax.psum_scatter(
        jnp.dot(hidden, narrowing_matrix, preferred_element_type=jnp.float32),
        ("kv", "tp"),
        scatter_dimension=1,
        tiled=True,
    )
    down_terms = (
        jnp.zeros((all_rows, mixer_terms.shape[1]), jnp.float32).at[live_order].set(mixer_terms)
    )
    mixed = jnp.where(live_rows[:, None], resid_wide + down_terms, 0.0).astype(jnp.bfloat16)
    return (mixed, carried)


def solution(mesh):
    placed = (
        P(None, ("kv", "tp")),
        P(),
        P("kv", "tp", None, None),
        P("kv"),
        P("kv", "tp"),
        P("kv", "tp"),
        P("kv", "tp"),
        P("kv", "tp"),
        P("tp"),
        P("kv", "tp"),
        P(),
        P("tp", "kv"),
        P(("kv", "tp")),
        P(None, ("kv", "tp")),
        P(None, ("kv", "tp")),
        P(("kv", "tp"), None),
    )
    return jax.shard_map(
        local,
        mesh=mesh,
        in_specs=placed,
        out_specs=(P(None, ("kv", "tp")), P("kv", "tp", None, None)),
        check_vma=False,
    )
```

profile of v0, /device:TPU:0, one launch (start us, length us, event | category | flops | bytes accessed | tf_op | source)
XLA Modules:
  0.0 449.3 jit_solution(15715938203859313457)
XLA Ops:
  7.2 0.0 copy-start
  7.2 0.0 copy-start.13
  7.2 0.0 reduce-scatter.10.cloned.1.call-start
  7.3 9.0 %all_gather.9 = bf16[512,512]{1,0:T(8,128)(2,1)S(1)} all-gather(bf16[512,128]{1,0:T(8,128)(2,1)} %param.16), channel_id=1, replica_groups=mesh['kv'=8,'tp'=4] {'tp'}, dimensions={1}, use_global_device_ids=true | all-gather | bytes 655360 | tf_op jit(solution)/shard_map/all_gather | solution.py:36
  16.3 1.6 convolution_convert_fusion.3
  17.9 0.5 convolution_convert_fusion.2
  18.4 0.5 convolution_convert_fusion.1
  18.9 0.5 convolution_convert_fusion.4
  19.4 1.5 pad_maximum_fusion
  20.8 4.0 copy.203
  24.8 0.0 copy-start.5
  24.8 0.0 reduce-scatter.10.cloned.1.call-update
  24.9 0.0 reduce-scatter.12.cloned.1.call-start
  24.9 0.5 copy-done.9
  25.5 0.1 dynamic_slice.6
  25.5 0.1 iota_compare_fusion.1
  25.6 0.1 lt.69
  25.7 0.1 add.123
  25.8 0.0 copy-done.3
  25.8 0.1 fusion.25
  26.0 40.8 %psum.14 = f32[512]{0:T(512)S(1)} all-reduce(f32[512]{0:T(512)S(1)} %fusion.25), channel_id=1, replica_groups=mesh['kv'=8,'tp'=4] {'kv','tp'}, use_global_device_ids=true, to_apply=%region_2.0 | all-reduce | flops 512 | bytes 4096 | tf_op jit(solution)/shard_map/psum | solution.py:37
  66.7 0.1 add_rsqrt_fusion.2
  66.8 28.5 %reduce-scatter.10.cloned.1.call-done = bf16[64,2048]{1,0:T(8,128)(2,1)} async-done(((bf16[512,2048]{1,0:T(8,128)(2,1)}), bf16[64,2048]{1,0:T(8,128)(2,1)}) %reduce-scatter.10.cloned.1.call-update) | async-done | bytes 262160 | tf_op jit(solution)/shard_map/reduce_scatter | solution.py:42
  95.3 1.2 convert_multiply_fusion
  96.6 0.2 fusion.55
  96.9 0.1 exponential_select_fusion
  97.0 0.2 fusion.56
  97.3 2.8 fusion
  100.1 4.3 fusion.18
  104.4 6.1 %fusion.1 = f32[8,4,1,128]{3,2,1,0:T(1,128)S(1)} fusion(f32[8,4,128]{2,1,0:T(4,128)S(1)} %bitcast.159, f32[8,4,128]{2,1,0:T(4,128)S(1)} %bitcast.183, f32[8,4,128]{2,1,0:T(4,128)S(1)} %bitcast.175, f32[8,4,128,128]{3,2,1,0:T(8,128)S(1)} %copy-done.1, f32[8,4,128]{2,1,0:T(4,128)S(1)} %bitcast.157, f32[8,4,128]{2,1,0:T(4,128)S(1)} %bitcast.181, ...), kind=kOutput, calls=%fused_computation.12 | convolution fusion | flops 11010048 | bytes 2277376 | tf_op jit(solution)/shard_map/bhd,bhdv->bhv/dot_general | solution.py:87
  110.5 9.0 %multiply_add_fusion = (f32[8,4,128,128]{3,2,1,0:T(8,128)S(1)}, f32[8,4,128,128]{3,2,1,0:T(8,128)S(1)}) fusion(f32[8,4,128]{2,1,0:T(4,128)S(1)} %bitcast.161, f32[8,4,128]{2,1,0:T(4,128)S(1)} %bitcast.185, f32[8,4,128]{2,1,0:T(4,128)S(1)} %bitcast.174, f32[8,4,128]{2,1,0:T(4,128)S(1)} %bitcast.154, f32[8,4,128]{2,1,0:T(4,128)S(1)} %bitcast.171, ...), kind=kLoop, calls=%fused_computation.3 | loop fusion | flops 12582912 | bytes 6684672 | tf_op jit(solution)/shard_map/add | solution.py:83
  119.5 6.1 %fusion.3 = f32[8,4,1,128]{3,2,1,0:T(1,128)S(1)} fusion(f32[8,4,128]{2,1,0:T(4,128)S(1)} %bitcast.155, f32[8,4,128]{2,1,0:T(4,128)S(1)} %bitcast.172, f32[8,4,128]{2,1,0:T(4,128)S(1)} %bitcast.170, f32[8,4,128,128]{3,2,1,0:T(8,128)S(1)} %get-tuple-element.5, f32[8,4,128]{2,1,0:T(4,128)S(1)} %bitcast.152, f32[8,4,128]{2,1,0:T(4,128)S(1)} %bitcast.167, ...), kind=kOutput, calls=%fused_computation.14 | convolution fusion | flops 11010048 | bytes 2277376 | tf_op jit(solution)/shard_map/bhd,bhdv->bhv/dot_general | solution.py:87
  125.6 4.3 fusion.19
  129.8 3.0 fusion.2
  132.8 1.9 fusion.49
  134.7 1.9 fusion.44
  136.6 0.1 multiply_reduce_fusion
  136.8 0.1 broadcast_multiply_fusion
  136.9 0.1 fusion.41
  137.0 0.0 copy-start.7
  137.0 31.3 %all_gather.10 = bf16[512,512]{1,0:T(8,128)(2,1)S(1)} all-gather(bf16[64,512]{1,0:T(8,128)(2,1)S(1)} %fusion.41), channel_id=1, replica_groups=mesh['kv'=8,'tp'=4] {'kv'}, dimensions={0}, use_global_device_ids=true | all-gather | bytes 589824 | tf_op jit(solution)/shard_map/all_gather | solution.py:103
  168.3 0.4 convolution_convert_fusion
  168.8 1.0 copy.205
  169.8 0.0 reduce-scatter.12.cloned.1.call-update
  169.8 0.0 all-gather.2.cloned.1.call-start
  169.8 0.1 iota_compare_fusion
  169.9 0.1 lt.64
  170.0 3.8 sort.17
  173.8 16.7 %reduce-scatter.12.cloned.1.call-done = bf16[128,512]{1,0:T(8,128)(2,1)} async-done(((bf16[512,512]{1,0:T(8,128)(2,1)}), bf16[128,512]{1,0:T(8,128)(2,1)}) %reduce-scatter.12.cloned.1.call-update) | async-done | bytes 131088
  190.6 1.0 copy.206
  191.6 0.2 fusion.29
  191.7 39.3 %psum.15 = f32[512]{0:T(512)S(1)} all-reduce(f32[512]{0:T(512)S(1)} %fusion.29), channel_id=1, replica_groups=mesh['kv'=8,'tp'=4] {'kv','tp'}, use_global_device_ids=true, to_apply=%region_7.8 | all-reduce | flops 512 | bytes 4096 | tf_op jit(solution)/shard_map/psum | solution.py:112
  231.1 0.1 fusion.28
  231.2 0.9 gather_fusion
  232.1 0.7 broadcast_select_fusion
  232.8 0.0 all-gather.2.cloned.1.call-update
  232.8 0.0 reduce-scatter.8.cloned.1.call-start
  232.9 53.8 %all-gather.2.cloned.1.call-done = bf16[256,4096]{1,0:T(8,128)(2,1)} async-done(((bf16[256,128]{1,0:T(8,128)(2,1)}), bf16[256,4096]{1,0:T(8,128)(2,1)}) %all-gather.2.cloned.1.call-update) | async-done | bytes 2097168 | tf_op jit(solution)/shard_map/all_gather | solution.py:121
  286.7 3.4 fusion.59
  290.1 8.0 %fusion.5 = f32[256,4096]{1,0:T(8,128)} fusion(bf16[344,4096]{1,0:T(8,128)(2,1)S(1)} %copy-done, bf16[256,4096]{1,0:T(8,128)(2,1)} %all-gather.2.cloned.1.call-done, bf16[4096,344]{0,1:T(8,128)(2,1)} %param.30, f32[256,344]{0,1:T(8,128)S(1)} %fusion.59), kind=kOutput, calls=%fused_computation.22 | convolution fusion | flops 1443368960 | bytes 12279808 | tf_op jit(solution)/shard_map/dot_general | solution.py:126
  298.1 0.0 reduce-scatter.8.cloned.1.call-update
  298.1 142.2 %reduce-scatter.8.cloned.1.call-done = f32[256,128]{1,0:T(8,128)} async-done(((f32[256,4096]{1,0:T(8,128)}), f32[256,128]{1,0:T(8,128)}) %reduce-scatter.8.cloned.1.call-update) | async-done | bytes 131088 | tf_op jit(solution)/shard_map/reduce_scatter | solution.py:125
  440.4 1.6 scatter_custom_fusion
  441.9 0.8 fusion.31
  (49 shorter events, 0.2 us)
Async XLA Ops:
  7.2 282.9 %copy-start = (bf16[344,4096]{1,0:T(8,128)(2,1)S(1)}, bf16[344,4096]{1,0:T(8,128)(2,1)}, u32[]{:S(2)}) copy-start(bf16[344,4096]{1,0:T(8,128)(2,1)} %param.31) | copy-start | bytes 8454148
  7.2 10.7 %copy-start.13 = (f32[512]{0:T(512)S(1)}, f32[512]{0:T(512)}, u32[]{:S(2)}) copy-start(f32[512]{0:T(512)} %param.19) | copy-start | bytes 6148
  7.2 10.7 %copy-start.10 = (bf16[512,512]{1,0:T(8,128)(2,1)S(1)}, bf16[512,512]{1,0:T(8,128)(2,1)}, u32[]{:S(2)}) copy-start(bf16[512,512]{1,0:T(8,128)(2,1)} %param.22) | copy-start | bytes 1572868
  7.2 88.1 %reduce-scatter.10.cloned.1.call-start = ((), (), s32[]{:S(2)}) async-start(), calls=%async_computation.5 | async-start | bytes 2359296 | tf_op jit(solution)/shard_map/reduce_scatter | solution.py:42
  7.2 11.1 %copy-start.11 = (bf16[512,512]{1,0:T(8,128)(2,1)S(1)}, bf16[512,512]{1,0:T(8,128)(2,1)}, u32[]{:S(2)}) copy-start(bf16[512,512]{1,0:T(8,128)(2,1)} %param.23) | copy-start | bytes 1572868
  16.3 2.6 copy-start.12
  24.8 0.7 copy-start.9
  24.8 0.9 copy-start.6
  24.8 1.0 copy-start.3
  24.8 42.0 %copy-start.8 = (f32[128]{0:T(128)S(1)}, f32[128]{0:T(128)}, u32[]{:S(2)}) copy-start(f32[128]{0:T(128)} %param.26) | copy-start | bytes 1540
  24.8 42.0 %copy-start.5 = (f32[512]{0:T(512)S(1)}, f32[512]{0:T(512)}, u32[]{:S(2)}) copy-start(f32[512]{0:T(512)} %param.24) | copy-start | bytes 6148
  24.9 165.7 %reduce-scatter.12.cloned.1.call-start = ((), (), s32[]{:S(2)}) async-start(), calls=%async_computation.6 | async-start | bytes 655360
  95.3 2.0 copy-start.1
  119.5 15.3 %copy-start.2 = (f32[8,4,128,128]{3,2,1,0:T(8,128)}, f32[8,4,128,128]{3,2,1,0:T(8,128)S(1)}, u32[]{:S(2)}) copy-start(f32[8,4,128,128]{3,2,1,0:T(8,128)S(1)} %get-tuple-element.4) | copy-start | bytes 6291460
  134.7 33.6 %copy-start.4 = (bf16[512,512]{1,0:T(8,128)(2,1)S(1)}, bf16[512,512]{1,0:T(8,128)(2,1)}, u32[]{:S(2)}) copy-start(bf16[512,512]{1,0:T(8,128)(2,1)} %param.27) | copy-start | bytes 1572868
  137.0 94.1 %copy-start.7 = (f32[128]{0:T(128)S(1)}, f32[128]{0:T(128)}, u32[]{:S(2)}) copy-start(f32[128]{0:T(128)} %param.28) | copy-start | bytes 1540
  169.8 116.9 %all-gather.2.cloned.1.call-start = ((), (), s32[]{:S(2)}) async-start(), calls=%async_computation.3 | async-start | bytes 2162688 | tf_op jit(solution)/shard_map/all_gather | solution.py:121
  232.8 207.5 %reduce-scatter.8.cloned.1.call-start = ((), (), s32[]{:S(2)}) async-start(), calls=%async_computation.4 | async-start | bytes 4325376 | tf_op jit(solution)/shard_map/reduce_scatter | solution.py:125
Sparse Core Ops, SparseCore 0:
  25.0 70.2 reduce-scatter.9
  169.9 20.6 reduce-scatter.11
  232.9 53.6 all-gather.1
  298.2 142.0 reduce-scatter.7
where the time goes:
time: 450 us; the launch traced here: 449 us
  waiting for transfers between devices  241 us (54%)
  blocking collectives  120 us (27%)
  matrix products  45.2 us (10%)
  other arithmetic  18.2 us (4%)
  between operations  14.2 us (3%)
  local copies, waits for them, and re-layouts  9.9 us (2%)
    reduce_scatter x1, waiting for transfers between devices, local(): lax.psum_scatter(jnp.dot(hidden, narrowing_matrix, preferred_element_type...  142 us
    all_gather x1, waiting for transfers between devices, local(): piece = lax.all_gather(mixer_input, ('kv', 'tp'), axis=1, tiled=True)  53.8 us
    psum x1, blocking collectives, local(): squares = lax.psum(jnp.sum(tokens_wide * tokens_wide, axis=1), ('kv', 'tp'))  40.8 us
    psum x1, blocking collectives, local(): lax.psum(jnp.sum(resid_wide * resid_wide, axis=1), ('kv', 'tp'))  39.3 us
    all_gather x1, blocking collectives, local(): lax.all_gather(normed, 'kv', axis=0, tiled=True)  31.3 us
    dot_general x8, matrix products, local(): jnp.einsum('bhd,bhdv->bhv', query[:, position], carried, precision=lax.Pr...  30.3 us
    reduce_scatter x1, waiting for transfers between devices, local(): lax.psum_scatter(jnp.concatenate([jnp.dot(scaled, weight, preferred_eleme...  28.5 us
    unnamed x5, waiting for transfers between devices  16.8 us
  transfers between devices with their start and end apart: 4, of which 4 were waited for; matrix products, arithmetic and copies ran while one was open for 1% of the time, Pallas kernels for 0%

commit v1 on v0

--- a/solution.py
+++ b/solution.py
@@ -34,7 +34,9 @@
     kv_index = lax.axis_index("kv")
     tokens_wide = residual_entries.astype(jnp.float32)
     columns = lax.all_gather(residual_entries, "tp", axis=1, tiled=True)
-    squares = lax.psum(jnp.sum(tokens_wide * tokens_wide, axis=1), ("kv", "tp"))
+    squares = jnp.sum(
+        lax.all_gather(jnp.sum(tokens_wide * tokens_wide, axis=1), ("kv", "tp")), axis=0
+    )
     own_squares = lax.dynamic_slice_in_dim(squares, kv_index * rows_dev, rows_dev)
     first_scale = lax.rsqrt(own_squares / D + epsilon)
     scaled = (columns.astype(jnp.float32) * initial_rescale_vector).astype(jnp.bfloat16)

time: 450 us -> 450 us (level)
    all_gather x0 -> x1, blocking collectives: none -> 41.9 us  [local(): lax.all_gather(jnp.sum(tokens_wide * tokens_wide, axis=1), ('kv', 'tp'))]
    psum x1 -> x0, blocking collectives: 40.8 us -> none  [local(): squares = lax.psum(jnp.sum(tokens_wide * tokens_wide, axis=1), ('kv', 'tp'))]
where the time goes in v1:
time: 450 us; the launch traced here: 449 us
  waiting for transfers between devices  240 us (53%)
  blocking collectives  121 us (27%)
  matrix products  45.2 us (10%)
  other arithmetic  18.2 us (4%)
  between operations  14.2 us (3%)
  local copies, waits for them, and re-layouts  9.9 us (2%)
    reduce_scatter x1, waiting for transfers between devices, local(): lax.psum_scatter(jnp.dot(hidden, narrowing_matrix, preferred_element_type...  142 us
    all_gather x1, waiting for transfers between devices, local(): piece = lax.all_gather(mixer_input, ('kv', 'tp'), axis=1, tiled=True)  53.9 us
    all_gather x1, blocking collectives, local(): lax.all_gather(jnp.sum(tokens_wide * tokens_wide, axis=1), ('kv', 'tp'))  41.9 us
    psum x1, blocking collectives, local(): lax.psum(jnp.sum(resid_wide * resid_wide, axis=1), ('kv', 'tp'))  39.3 us
    all_gather x1, blocking collectives, local(): lax.all_gather(normed, 'kv', axis=0, tiled=True)  31.3 us
    dot_general x8, matrix products, local(): jnp.einsum('bhd,bhdv->bhv', query[:, position], carried, precision=lax.Pr...  30.3 us
    reduce_scatter x1, waiting for transfers between devices, local(): lax.psum_scatter(jnp.concatenate([jnp.dot(scaled, weight, preferred_eleme...  27.1 us
    unnamed x5, waiting for transfers between devices  16.6 us
  transfers between devices with their start and end apart: 4, of which 4 were waited for; matrix products, arithmetic and copies ran while one was open for 1% of the time, Pallas kernels for 0%

profile of v1, /device:TPU:0, one launch (start us, length us, event | category | flops | bytes accessed | tf_op | source)
XLA Modules:
  0.0 449.2 jit_solution(8770353345134961623)
XLA Ops:
  7.2 0.0 copy-start
  7.2 0.0 copy-start.13
  7.2 0.0 reduce-scatter.10.cloned.1.call-start
  7.3 9.0 %all_gather.15 = bf16[512,512]{1,0:T(8,128)(2,1)S(1)} all-gather(bf16[512,128]{1,0:T(8,128)(2,1)} %param.16), channel_id=1, replica_groups=mesh['kv'=8,'tp'=4] {'tp'}, dimensions={1}, use_global_device_ids=true | all-gather | bytes 655360 | tf_op jit(solution)/shard_map/all_gather | solution.py:36
  16.3 1.6 convolution_convert_fusion.3
  17.9 0.5 convolution_convert_fusion.2
  18.4 0.5 convolution_convert_fusion.1
  18.9 0.5 convolution_convert_fusion.4
  19.4 1.5 pad_maximum_fusion
  20.8 4.0 copy.203
  24.8 0.0 copy-start.5
  24.8 0.0 reduce-scatter.10.cloned.1.call-update
  24.9 0.0 reduce-scatter.12.cloned.1.call-start
  24.9 0.5 copy-done.9
  25.5 0.1 dynamic_slice.6
  25.5 0.1 iota_compare_fusion.1
  25.6 0.1 lt.69
  25.7 0.1 add.121
  25.8 0.1 fusion.25
  26.0 41.9 %all-gather.1 = f32[32,1,512]{2,1,0:T(1,128)S(1)} all-gather(f32[1,1,512]{2,1,0:T(1,128)S(1)} %bitcast.196), channel_id=2, replica_groups=mesh['kv'=8,'tp'=4] {'kv','tp'}, dimensions={0}, use_global_device_ids=true | all-gather | bytes 67584 | tf_op jit(solution)/shard_map/all_gather | solution.py:38
  67.8 0.1 reduce_sum.37
  67.9 0.1 add_rsqrt_fusion.2
  68.0 27.1 %reduce-scatter.10.cloned.1.call-done = bf16[64,2048]{1,0:T(8,128)(2,1)} async-done(((bf16[512,2048]{1,0:T(8,128)(2,1)}), bf16[64,2048]{1,0:T(8,128)(2,1)}) %reduce-scatter.10.cloned.1.call-update) | async-done | bytes 262160 | tf_op jit(solution)/shard_map/reduce_scatter | solution.py:44
  95.1 1.2 convert_multiply_fusion
  96.4 0.2 fusion.55
  96.7 0.1 exponential_select_fusion
  96.8 0.2 fusion.56
  97.1 3.0 fusion
  100.1 4.3 fusion.18
  104.3 6.1 %fusion.1 = f32[8,4,1,128]{3,2,1,0:T(1,128)S(1)} fusion(f32[8,4,128]{2,1,0:T(4,128)S(1)} %bitcast.160, f32[8,4,128]{2,1,0:T(4,128)S(1)} %bitcast.184, f32[8,4,128]{2,1,0:T(4,128)S(1)} %bitcast.176, f32[8,4,128,128]{3,2,1,0:T(8,128)S(1)} %copy-done.1, f32[8,4,128]{2,1,0:T(4,128)S(1)} %bitcast.158, f32[8,4,128]{2,1,0:T(4,128)S(1)} %bitcast.182, ...), kind=kOutput, calls=%fused_computation.12 | convolution fusion | flops 11010048 | bytes 2277376 | tf_op jit(solution)/shard_map/bhd,bhdv->bhv/dot_general | solution.py:89
  110.4 9.0 %multiply_add_fusion = (f32[8,4,128,128]{3,2,1,0:T(8,128)S(1)}, f32[8,4,128,128]{3,2,1,0:T(8,128)S(1)}) fusion(f32[8,4,128]{2,1,0:T(4,128)S(1)} %bitcast.162, f32[8,4,128]{2,1,0:T(4,128)S(1)} %bitcast.186, f32[8,4,128]{2,1,0:T(4,128)S(1)} %bitcast.175, f32[8,4,128]{2,1,0:T(4,128)S(1)} %bitcast.155, f32[8,4,128]{2,1,0:T(4,128)S(1)} %bitcast.172, ...), kind=kLoop, calls=%fused_computation.3 | loop fusion | flops 12582912 | bytes 6684672 | tf_op jit(solution)/shard_map/add | solution.py:85
  119.4 6.1 %fusion.3 = f32[8,4,1,128]{3,2,1,0:T(1,128)S(1)} fusion(f32[8,4,128]{2,1,0:T(4,128)S(1)} %bitcast.156, f32[8,4,128]{2,1,0:T(4,128)S(1)} %bitcast.173, f32[8,4,128]{2,1,0:T(4,128)S(1)} %bitcast.171, f32[8,4,128,128]{3,2,1,0:T(8,128)S(1)} %get-tuple-element.5, f32[8,4,128]{2,1,0:T(4,128)S(1)} %bitcast.153, f32[8,4,128]{2,1,0:T(4,128)S(1)} %bitcast.168, ...), kind=kOutput, calls=%fused_computation.14 | convolution fusion | flops 11010048 | bytes 2277376 | tf_op jit(solution)/shard_map/bhd,bhdv->bhv/dot_general | solution.py:89
  125.5 4.3 fusion.19
  129.8 2.8 fusion.2
  132.6 1.9 fusion.49
  134.5 1.9 fusion.44
  136.4 0.1 multiply_reduce_fusion
  136.6 0.1 broadcast_multiply_fusion
  136.7 0.1 fusion.41
  136.8 0.0 copy-start.7
  136.8 31.3 %all_gather.18 = bf16[512,512]{1,0:T(8,128)(2,1)S(1)} all-gather(bf16[64,512]{1,0:T(8,128)(2,1)S(1)} %fusion.41), channel_id=1, replica_groups=mesh['kv'=8,'tp'=4] {'kv'}, dimensions={0}, use_global_device_ids=true | all-gather | bytes 589824 | tf_op jit(solution)/shard_map/all_gather | solution.py:105
  168.1 0.4 convolution_convert_fusion
  168.5 1.0 copy.205
  169.5 0.0 reduce-scatter.12.cloned.1.call-update
  169.6 0.3 all-gather.4.cloned.1.call-start
  169.8 0.1 iota_compare_fusion
  169.9 0.1 lt.64
  170.0 3.8 sort.17
  173.8 16.5 %reduce-scatter.12.cloned.1.call-done = bf16[128,512]{1,0:T(8,128)(2,1)} async-done(((bf16[512,512]{1,0:T(8,128)(2,1)}), bf16[128,512]{1,0:T(8,128)(2,1)}) %reduce-scatter.12.cloned.1.call-update) | async-done | bytes 131088
  190.4 1.0 copy.206
  191.4 0.2 fusion.29
  191.5 39.3 %psum.7 = f32[512]{0:T(512)S(1)} all-reduce(f32[512]{0:T(512)S(1)} %fusion.29), channel_id=1, replica_groups=mesh['kv'=8,'tp'=4] {'kv','tp'}, use_global_device_ids=true, to_apply=%region_7.8 | all-reduce | flops 512 | bytes 4096 | tf_op jit(solution)/shard_map/psum | solution.py:114
  230.9 0.1 fusion.28
  231.0 0.9 gather_fusion
  231.9 0.7 broadcast_select_fusion
  232.6 0.0 all-gather.4.cloned.1.call-update
  232.6 0.0 reduce-scatter.8.cloned.1.call-start
  232.7 53.9 %all-gather.4.cloned.1.call-done = bf16[256,4096]{1,0:T(8,128)(2,1)} async-done(((bf16[256,128]{1,0:T(8,128)(2,1)}), bf16[256,4096]{1,0:T(8,128)(2,1)}) %all-gather.4.cloned.1.call-update) | async-done | bytes 2097168 | tf_op jit(solution)/shard_map/all_gather | solution.py:123
  286.5 3.4 fusion.59
  289.9 8.0 %fusion.5 = f32[256,4096]{1,0:T(8,128)} fusion(bf16[344,4096]{1,0:T(8,128)(2,1)S(1)} %copy-done, bf16[256,4096]{1,0:T(8,128)(2,1)} %all-gather.4.cloned.1.call-done, bf16[4096,344]{0,1:T(8,128)(2,1)} %param.30, f32[256,344]{0,1:T(8,128)S(1)} %fusion.59), kind=kOutput, calls=%fused_computation.22 | convolution fusion | flops 1443368960 | bytes 12279808 | tf_op jit(solution)/shard_map/dot_general | solution.py:128
  298.0 0.0 reduce-scatter.8.cloned.1.call-update
  298.0 142.3 %reduce-scatter.8.cloned.1.call-done = f32[256,128]{1,0:T(8,128)} async-done(((f32[256,4096]{1,0:T(8,128)}), f32[256,128]{1,0:T(8,128)}) %reduce-scatter.8.cloned.1.call-update) | async-done | bytes 131088 | tf_op jit(solution)/shard_map/reduce_scatter | solution.py:127
  440.3 1.6 scatter_custom_fusion
  441.9 0.8 fusion.31
  (50 shorter events, 0.2 us)
Async XLA Ops:
  7.2 282.8 %copy-start = (bf16[344,4096]{1,0:T(8,128)(2,1)S(1)}, bf16[344,4096]{1,0:T(8,128)(2,1)}, u32[]{:S(2)}) copy-start(bf16[344,4096]{1,0:T(8,128)(2,1)} %param.31) | copy-start | bytes 8454148
  7.2 10.7 %copy-start.13 = (f32[512]{0:T(512)S(1)}, f32[512]{0:T(512)}, u32[]{:S(2)}) copy-start(f32[512]{0:T(512)} %param.19) | copy-start | bytes 6148
  7.2 10.7 %copy-start.10 = (bf16[512,512]{1,0:T(8,128)(2,1)S(1)}, bf16[512,512]{1,0:T(8,128)(2,1)}, u32[]{:S(2)}) copy-start(bf16[512,512]{1,0:T(8,128)(2,1)} %param.22) | copy-start | bytes 1572868
  7.2 87.9 %reduce-scatter.10.cloned.1.call-start = ((), (), s32[]{:S(2)}) async-start(), calls=%async_computation.5 | async-start | bytes 2359296 | tf_op jit(solution)/shard_map/reduce_scatter | solution.py:44
  7.2 11.1 %copy-start.11 = (bf16[512,512]{1,0:T(8,128)(2,1)S(1)}, bf16[512,512]{1,0:T(8,128)(2,1)}, u32[]{:S(2)}) copy-start(bf16[512,512]{1,0:T(8,128)(2,1)} %param.23) | copy-start | bytes 1572868
  16.3 2.6 copy-start.12
  24.8 0.7 copy-start.9
  24.8 0.9 copy-start.6
  24.8 1.0 copy-start.3
  24.8 43.2 %copy-start.8 = (f32[128]{0:T(128)S(1)}, f32[128]{0:T(128)}, u32[]{:S(2)}) copy-start(f32[128]{0:T(128)} %param.26) | copy-start | bytes 1540
  24.8 43.2 %copy-start.5 = (f32[512]{0:T(512)S(1)}, f32[512]{0:T(512)}, u32[]{:S(2)}) copy-start(f32[512]{0:T(512)} %param.24) | copy-start | bytes 6148
  24.9 165.5 %reduce-scatter.12.cloned.1.call-start = ((), (), s32[]{:S(2)}) async-start(), calls=%async_computation.6 | async-start | bytes 655360
  95.1 2.0 copy-start.1
  119.4 15.1 %copy-start.2 = (f32[8,4,128,128]{3,2,1,0:T(8,128)}, f32[8,4,128,128]{3,2,1,0:T(8,128)S(1)}, u32[]{:S(2)}) copy-start(f32[8,4,128,128]{3,2,1,0:T(8,128)S(1)} %get-tuple-element.4) | copy-start | bytes 6291460
  134.5 33.6 %copy-start.4 = (bf16[512,512]{1,0:T(8,128)(2,1)S(1)}, bf16[512,512]{1,0:T(8,128)(2,1)}, u32[]{:S(2)}) copy-start(bf16[512,512]{1,0:T(8,128)(2,1)} %param.27) | copy-start | bytes 1572868
  136.8 94.1 %copy-start.7 = (f32[128]{0:T(128)S(1)}, f32[128]{0:T(128)}, u32[]{:S(2)}) copy-start(f32[128]{0:T(128)} %param.28) | copy-start | bytes 1540
  169.6 117.0 %all-gather.4.cloned.1.call-start = ((), (), s32[]{:S(2)}) async-start(), calls=%async_computation.3 | async-start | bytes 2162688 | tf_op jit(solution)/shard_map/all_gather | solution.py:123
  232.6 207.7 %reduce-scatter.8.cloned.1.call-start = ((), (), s32[]{:S(2)}) async-start(), calls=%async_computation.4 | async-start | bytes 4325376 | tf_op jit(solution)/shard_map/reduce_scatter | solution.py:127
Sparse Core Ops, SparseCore 0:
  25.0 70.0 reduce-scatter.9
  169.7 20.6 reduce-scatter.11
  232.7 53.7 all-gather.3
  298.1 142.1 reduce-scatter.7
